TPU v7x, 32 devices: a whole 2x2x4 slice. The times are simulated.
32 devices in a mesh: sp: 4 (over x, core), dp: 8 (over z, y).
Axes of the slice: x: 2, y: 2, z: 4, core: 2. Of those that a mesh axis runs over, the one named last changes fastest.
Arguments:
- tokens: bfloat16 [8, 1536, 2048], P('dp', 'sp'), may hold values from -6 to 6
- w_value: bfloat16 [2048, 1024], P('dp'), may hold values from -0.125 to 0.125
- w_gate: bfloat16 [2048, 1024], P('dp'), may hold values from -0.125 to 0.125
- conv_taps: bfloat16 [31, 1024], replicated, may hold values from -1 to 1
- norm_gain: bfloat16 [1024], replicated, may hold values from 0.099609375 to 1.8984375
- w_out: bfloat16 [1024, 2048], P(None, 'dp'), may hold values from -0.1875 to 0.1875
Outputs:
- mixed: bfloat16 [8, 1536, 2048], P('dp', 'sp')
All inputs are finite; a program needn't handle non-finite values.
Results may differ from a plain program's by a relative error of at most 0.013.
Values may be sent and summed in bfloat16 or wider, within the bound.
No kernel may reach another device: no remote copies, remote signals or barrier semaphores. Data moves between devices by JAX's collectives and lax.ppermute only.
A program may use at most 64 MiB of HBM per device.

v0:
```python
import jax
import jax.numpy as jnp
from jax import lax
from jax.sharding import PartitionSpec as P

EPSILON = 1e-06


def passed_along(x, axis, by):
    length = lax.axis_size(axis)
    pairs = [(i, i + by) for i in range(length) if 0 <= i + by < length]
    return lax.ppermute(x, axis, pairs)


def depthwise_conv(signal, local_taps, left_pad):
    kernel_form = jnp.transpose(local_taps)[:, None, :]
    result = lax.conv_general_dilated(
        signal[None],
        kernel_form,
        (1,),
        [(left_pad, 0)],
        dimension_numbers=("NCH", "OIH", "NCH"),
        feature_group_count=signal.shape[0],
        preferred_element_type=jnp.float32,
    )
    return result[0].astype(jnp.bfloat16)


def body(tokens, w_value, w_gate, conv_taps, norm_gain, w_out):
    seq_rows = tokens[0]
    tok_count = seq_rows.shape[0]
    kernel_len = conv_taps.shape[0]
    value_sum = jnp.einsum(
        "dc,td->ct",
        lax.all_gather(w_value, "dp", axis=0, tiled=True),
        seq_rows,
        preferred_element_type=jnp.float32,
    )
    gate_sum = jnp.einsum(
        "dc,td->ct",
        lax.all_gather(w_gate, "dp", axis=0, tiled=True),
        seq_rows,
        preferred_element_type=jnp.float32,
    )
    gated = (value_sum * jax.nn.sigmoid(gate_sum)).astype(jnp.bfloat16)
    last_rows = gated[:, tok_count - (kernel_len - 1) :]
    earlier = passed_along(last_rows, "sp", 1)
    extended = jnp.concatenate([earlier, gated], axis=1)
    conv_out = depthwise_conv(extended, conv_taps, 0)
    wide = conv_out.astype(jnp.float32)
    chan_mean = jnp.mean(wide, 0, keepdims=True)
    centred = wide - chan_mean
    chan_var = jnp.mean(centred * centred, 0, keepdims=True)
    normed = centred * lax.rsqrt(chan_var + EPSILON) * norm_gain.astype(jnp.float32)[:, None]
    activated = (normed * jax.nn.sigmoid(normed)).astype(jnp.bfloat16)
    projected = jnp.einsum(
        "ct,cd->td",
        activated,
        lax.all_gather(w_out, "dp", axis=1, tiled=True),
        preferred_element_type=jnp.float32,
    ).astype(jnp.bfloat16)
    return projected[None]


def solution(mesh):
    placed = (P("dp", "sp", None), P("dp", None), P("dp", None), P(), P(), P(None, "dp"))
    return jax.shard_map(
        body, mesh=mesh, in_specs=placed, out_specs=P("dp", "sp", None), check_vma=False
    )
```

profile of v0, /device:TPU:0, one launch (start us, length us, event | category | flops | bytes accessed | tf_op | source)
XLA Modules:
  0.0 246.4 jit_solution(6799378059922831921)
XLA Ops:
  6.5 0.7 all-gather.6.cloned.1.call-update
  7.3 0.0 all-gather.4.cloned.1.call-start
  7.3 0.7 all-gather.4.cloned.1.call-update
  8.0 0.0 all-gather.8.cloned.1.call-start
  8.1 0.7 all-gather.8.cloned.1.call-update
  8.7 76.3 %all-gather.6.cloned.1.call-done = bf16[2048,1024]{1,0:T(8,128)(2,1)} async-done(((bf16[256,1024]{1,0:T(8,128)(2,1)}), bf16[2048,1024]{1,0:T(8,128)(2,1)}) %all-gather.6.cloned.1.call-update) | async-done | bytes 4194320 | tf_op jit(solution)/shard_map/all_gather | solution.py:41
  85.0 4.0 %fusion.4 = f32[1024,384]{0,1:T(8,128)S(1)} fusion(bf16[2048,1024]{1,0:T(8,128)(2,1)} %all-gather.6.cloned.1.call-done, bf16[1,384,2048]{2,1,0:T(8,128)(2,1)S(1)} %copy-done), kind=kOutput, calls=%fused_computation.8 | convolution fusion | flops 1610612736 | bytes 7340032 | tf_op jit(solution)/shard_map/dc,td->ct/dot_general | solution.py:39
  89.0 69.5 %all-gather.4.cloned.1.call-done = bf16[2048,1024]{1,0:T(8,128)(2,1)} async-done(((bf16[256,1024]{1,0:T(8,128)(2,1)}), bf16[2048,1024]{1,0:T(8,128)(2,1)}) %all-gather.4.cloned.1.call-update) | async-done | bytes 4194320 | tf_op jit(solution)/shard_map/all_gather | solution.py:35
  158.5 4.1 %multiply_convert_fusion.1 = bf16[1024,384]{0,1:T(8,128)(2,1)S(1)} fusion(f32[1024,384]{0,1:T(8,128)S(1)} %fusion.4, bf16[2048,1024]{1,0:T(8,128)(2,1)} %all-gather.4.cloned.1.call-done, bf16[1,384,2048]{2,1,0:T(8,128)(2,1)S(1)} %copy-done), kind=kOutput, calls=%fused_computation.12 | convolution fusion | flops 1612578816 | bytes 8126464 | tf_op jit(solution)/shard_map/dc,td->ct/dot_general | solution.py:33
  162.6 1.3 collective-permute-start
  163.9 0.9 collective-permute-done
  164.8 0.2 maximum_bitcast_fusion
  165.0 0.1 pad
  165.0 0.2 reshape.17
  165.2 0.5 copy.12
  165.7 0.1 slice.7
  165.8 0.2 copy-done.2
  166.0 3.8 %fusion.17 = f32[8,52,1024]{2,0,1:T(8,128)S(1)} fusion(bf16[1024,1,7,30]{0,2,3,1:T(8,128)(2,1)S(1)} %slice.7, bf16[1024,1,8,52]{0,2,3,1:T(8,128)(2,1)S(1)} %copy.12, pred[8,52]{0,1:T(8,128)(4,1)S(1)} %copy-done.3, bf16[1024,1,31]{0,2,1:T(8,128)(2,1)S(1)} %bitcast.35), kind=kOutput, calls=%fused_computation.20 | convolution fusion | flops 31719424 | bytes 3049888 | tf_op jit(solution)/shard_map/conv_general_dilated | solution.py:17
  169.8 2.2 copy.14
  172.1 1.6 reshape.21
  173.7 0.2 slice_reduce_fusion
  173.8 0.3 multiply_reduce_fusion
  174.1 60.3 %all-gather.8.cloned.1.call-done = bf16[1024,2048]{1,0:T(8,128)(2,1)} async-done(((bf16[1024,256]{1,0:T(8,128)(2,1)}), bf16[1024,2048]{1,0:T(8,128)(2,1)}) %all-gather.8.cloned.1.call-update) | async-done | bytes 4194320 | tf_op jit(solution)/shard_map/all_gather | solution.py:59
  234.5 5.5 %fusion.1 = bf16[1,384,2048]{2,1,0:T(8,128)(2,1)} fusion(bf16[1024,2048]{1,0:T(8,128)(2,1)} %all-gather.8.cloned.1.call-done, f32[1,416,1024]{2,1,0:T(8,128)S(1)} %reshape.21, f32[1024]{0:T(1024)S(1)} %convert_element_type.26, f32[384]{0:T(512)S(1)} %add_rsqrt_fusion, f32[384]{0:T(512)S(1)} %broadcast_multiply_fusion), kind=kOutput, calls=%fused_computation.3 | convolution fusion | flops 1614544896 | bytes 7348224 | tf_op jit(solution)/shard_map/ct,cd->td/dot_general | solution.py:56
  (12 shorter events, 0.1 us)
Async XLA Ops:
  6.5 78.5 %copy-start = (bf16[1,384,2048]{2,1,0:T(8,128)(2,1)S(1)}, bf16[1,384,2048]{2,1,0:T(8,128)(2,1)}, u32[]{:S(2)}) copy-start(bf16[1,384,2048]{2,1,0:T(8,128)(2,1)} %param.6) | copy-start | bytes 4718596
  6.5 78.5 %all-gather.6.cloned.1.call-start = ((), (), s32[]{:S(2)}) async-start(), calls=%async_computation.1 | async-start | bytes 4718592 | tf_op jit(solution)/shard_map/all_gather | solution.py:41
  7.3 151.2 %all-gather.4.cloned.1.call-start = ((), (), s32[]{:S(2)}) async-start(), calls=%async_computation | async-start | bytes 4718592 | tf_op jit(solution)/shard_map/all_gather | solution.py:35
  8.0 226.4 %all-gather.8.cloned.1.call-start = ((), (), s32[]{:S(2)}) async-start(), calls=%async_computation.2 | async-start | bytes 4718592 | tf_op jit(solution)/shard_map/all_gather | solution.py:59
  89.0 74.9 %copy-start.1 = (bf16[1024]{0:T(1024)(128)(2,1)S(1)}, bf16[1024]{0:T(1024)(128)(2,1)}, u32[]{:S(2)}) copy-start(bf16[1024]{0:T(1024)(128)(2,1)} %param.10) | copy-start | bytes 6148
  162.6 2.2 collective-permute-start
  165.2 0.8 copy-start.2
  165.2 0.8 copy-start.3
Sparse Core Ops, SparseCore 0:
  9.5 75.5 all-gather.5
  87.1 71.3 all-gather.3
  160.5 73.8 all-gather.7
where the time goes:
time: 247 us; the launch traced here: 246 us
  waiting for transfers between devices  209 us (85%)
  matrix products  17.3 us (7%)
  between operations  13.2 us (5%)
  local copies, waits for them, and re-layouts  4.87 us (2%)
    all_gather x1, waiting for transfers between devices, body(): lax.all_gather(w_gate, 'dp', axis=0, tiled=True)  76.3 us
    all_gather x1, waiting for transfers between devices, body(): lax.all_gather(w_value, 'dp', axis=0, tiled=True)  69.5 us
    all_gather x1, waiting for transfers between devices, body(): lax.all_gather(w_out, 'dp', axis=1, tiled=True)  60.3 us
    dot_general x1, matrix products, body(): jnp.einsum('ct,cd->td', activated, lax.all_gather(w_out, 'dp', axis=1, ti...  5.46 us
  transfers between devices with their start and end apart: 4, of which 4 were waited for; matrix products, arithmetic and copies ran while one was open for 7% of the time, Pallas kernels for 0%

commit v1 on v0

--- a/solution.py
+++ b/solution.py
@@ -2,6 +2,7 @@
 import jax.numpy as jnp
 from jax import lax
 from jax.sharding import PartitionSpec as P
+from jax.lax import axis_index, axis_size, ppermute
 
 EPSILON = 1e-06
 
@@ -27,6 +28,22 @@
 
 
 def body(tokens, w_value, w_gate, conv_taps, norm_gain, w_out):
+
+    def fix_the_loops(here_x, bus_axis, vector):
+        z2, x_new, step_out = (axis_size(bus_axis), axis_index(bus_axis), here_x.shape[1])
+        pool = tuple(((dev_j, (dev_j + 1) % z2) for dev_j in range(z2)))
+        m_next, v_next = (here_x, None)
+        for tick in range(z2):
+            all_rows = (x_new - tick) % z2
+            left_arr = ppermute(m_next, bus_axis, perm=pool) if tick < z2 - 1 else None
+            g_now = vector(m_next, all_rows * step_out)
+            f_next = g_now.shape[1]
+            if v_next is None:
+                v_next = jnp.zeros((*g_now.shape[:1], z2 * f_next, *g_now.shape[2:]), g_now.dtype)
+            v_next = lax.dynamic_update_slice_in_dim(v_next, g_now, all_rows * f_next, axis=1)
+            m_next = left_arr
+        return v_next
+
     seq_rows = tokens[0]
     tok_count = seq_rows.shape[0]
     kernel_len = conv_taps.shape[0]
@@ -53,11 +70,12 @@
     chan_var = jnp.mean(centred * centred, 0, keepdims=True)
     normed = centred * lax.rsqrt(chan_var + EPSILON) * norm_gain.astype(jnp.float32)[:, None]
     activated = (normed * jax.nn.sigmoid(normed)).astype(jnp.bfloat16)
-    projected = jnp.einsum(
-        "ct,cd->td",
-        activated,
-        lax.all_gather(w_out, "dp", axis=1, tiled=True),
-        preferred_element_type=jnp.float32,
+    projected = fix_the_loops(
+        w_out,
+        "dp",
+        lambda part, start: jnp.einsum(
+            "ct,cd->td", activated, part, preferred_element_type=jnp.float32
+        ),
     ).astype(jnp.bfloat16)
     return projected[None]
 

time: 247 us -> 234 us (0.947)
  waiting for transfers between devices: 209 us -> 182 us
  local copies, waits for them, and re-layouts: 4.87 us -> 10.6 us
  starting transfers between devices: 1.37 us -> 6.27 us
    ppermute x0 -> x7, waiting for transfers between devices: none -> 113 us  [fix_the_loops(): left_arr = ppermute(m_next, bus_axis, perm=pool) if tick < z2 - 1 else None]
    all_gather x1, waiting for transfers between devices: 76.3 us -> 0.01 us  [body(): lax.all_gather(w_gate, 'dp', axis=0, tiled=True)]
    all_gather x1 -> x0, waiting for transfers between devices: 60.3 us -> none  [body(): lax.all_gather(w_out, 'dp', axis=1, tiled=True)]
    unnamed x8 -> x32, local copies, waits for them, and re-layouts: 0.25 us -> 5.81 us
    ppermute x0 -> x7, starting transfers between devices: none -> 4.94 us  [fix_the_loops(): left_arr = ppermute(m_next, bus_axis, perm=pool) if tick < z2 - 1 else None]
    dot_general x1 -> x8, matrix products: 5.46 us -> 5.09 us  [body(): jnp.einsum('ct,cd->td', activated, part, preferred_element_type=jnp.float32)]
  transfers between devices with their start and end apart: 4 -> 10, of which waited for: 4 -> 7; matrix products, arithmetic and copies ran while one was open for 7% -> 10% of each run, Pallas kernels for 0% -> 0%
where the time goes in v1:
time: 234 us; the launch traced here: 233 us
  waiting for transfers between devices  182 us (78%)
  matrix products  18.8 us (8%)
  between operations  13.8 us (6%)
  local copies, waits for them, and re-layouts  10.6 us (5%)
  starting transfers between devices  6.27 us (3%)
    ppermute x7, waiting for transfers between devices, fix_the_loops(): left_arr = ppermute(m_next, bus_axis, perm=pool) if tick < z2 - 1 else None  113 us
    all_gather x1, waiting for transfers between devices, body(): lax.all_gather(w_value, 'dp', axis=0, tiled=True)  67.6 us
    unnamed x32, local copies, waits for them, and re-layouts  5.81 us
    dot_general x1, matrix products, body(): jnp.einsum('dc,td->ct', lax.all_gather(w_gate, 'dp', axis=0, tiled=True),...  5.38 us
    dot_general x8, matrix products, body(): jnp.einsum('ct,cd->td', activated, part, preferred_element_type=jnp.float32)  5.09 us
    ppermute x7, starting transfers between devices, fix_the_loops(): left_arr = ppermute(m_next, bus_axis, perm=pool) if tick < z2 - 1 else None  4.94 us
  transfers between devices with their start and end apart: 10, of which 7 were waited for; matrix products, arithmetic and copies ran while one was open for 10% of the time, Pallas kernels for 0%

profile of v1, /device:TPU:0, one launch (start us, length us, event | category | flops | bytes accessed | tf_op | source)
XLA Modules:
  0.0 232.7 jit_solution(2550943828507368246)
XLA Ops:
  6.5 0.7 all-gather.5.cloned.1.call-update
  8.0 3.0 %collective-permute-start.1 = (bf16[1024,256]{1,0:T(8,128)(2,1)}, bf16[1024,256]{1,0:T(8,128)(2,1)S(1)}, u32[]{:S(2)}, u32[]{:S(2)}) collective-permute-start(bf16[1024,256]{1,0:T(8,128)(2,1)} %param.11), channel_id=1, source_target_pairs={{0,1},{1,2},{2,3},{3,4},{4,5},{5,6},{6,7},{7,0},{8,9},{9,10},{10,1... | collective-permute-start | bytes 1572872 | tf_op jit(solution)/shard_map/ppermute | solution.py:38
  11.1 15.5 %collective-permute-done.1 = bf16[1024,256]{1,0:T(8,128)(2,1)S(1)} collective-permute-done((bf16[1024,256]{1,0:T(8,128)(2,1)}, bf16[1024,256]{1,0:T(8,128)(2,1)S(1)}, u32[]{:S(2)}, u32[]{:S(2)}) %collective-permute-start.1) | collective-permute-done | bytes 524320 | tf_op jit(solution)/shard_map/ppermute | solution.py:38
  26.6 0.9 copy-done.3
  27.5 1.1 collective-permute-start.2
  28.5 25.8 %collective-permute-done.2 = bf16[1024,256]{1,0:T(8,128)(2,1)S(1)} collective-permute-done((bf16[1024,256]{1,0:T(8,128)(2,1)S(1)}, bf16[1024,256]{1,0:T(8,128)(2,1)S(1)}, u32[]{:S(2)}, u32[]{:S(2)}) %collective-permute-start.2) | collective-permute-done | bytes 524320 | tf_op jit(solution)/shard_map/ppermute | solution.py:38
  54.4 0.8 copy-done.5
  55.2 27.0 %collective-permute-done.3 = bf16[1024,256]{1,0:T(8,128)(2,1)S(1)} collective-permute-done((bf16[1024,256]{1,0:T(8,128)(2,1)S(1)}, bf16[1024,256]{1,0:T(8,128)(2,1)S(1)}, u32[]{:S(2)}, u32[]{:S(2)}) %collective-permute-start.3) | collective-permute-done | bytes 524320 | tf_op jit(solution)/shard_map/ppermute | solution.py:38
  82.2 0.8 copy-done.7
  83.0 26.9 %collective-permute-done.4 = bf16[1024,256]{1,0:T(8,128)(2,1)S(1)} collective-permute-done((bf16[1024,256]{1,0:T(8,128)(2,1)S(1)}, bf16[1024,256]{1,0:T(8,128)(2,1)S(1)}, u32[]{:S(2)}, u32[]{:S(2)}) %collective-permute-start.4) | collective-permute-done | bytes 524320 | tf_op jit(solution)/shard_map/ppermute | solution.py:38
  109.8 0.8 copy-done.9
  110.6 16.7 %collective-permute-done.5 = bf16[1024,256]{1,0:T(8,128)(2,1)S(1)} collective-permute-done((bf16[1024,256]{1,0:T(8,128)(2,1)S(1)}, bf16[1024,256]{1,0:T(8,128)(2,1)S(1)}, u32[]{:S(2)}, u32[]{:S(2)}) %collective-permute-start.5) | collective-permute-done | bytes 524320 | tf_op jit(solution)/shard_map/ppermute | solution.py:38
  127.4 5.4 %fusion.3 = f32[1024,384]{0,1:T(8,128)} fusion(bf16[2048,1024]{1,0:T(8,128)(2,1)} %all-gather.5.cloned.1.call-done, bf16[1,384,2048]{2,1,0:T(8,128)(2,1)S(1)} %copy-done), kind=kOutput, calls=%fused_computation.6 | convolution fusion | flops 1610612736 | bytes 7340032 | tf_op jit(solution)/shard_map/dc,td->ct/dot_general | solution.py:56
  132.7 67.6 %all-gather.3.cloned.1.call-done = bf16[2048,1024]{1,0:T(8,128)(2,1)} async-done(((bf16[256,1024]{1,0:T(8,128)(2,1)}), bf16[2048,1024]{1,0:T(8,128)(2,1)}) %all-gather.3.cloned.1.call-update) | async-done | bytes 4194320 | tf_op jit(solution)/shard_map/all_gather | solution.py:52
  200.4 4.5 %multiply_convert_fusion.1 = bf16[1024,384]{0,1:T(8,128)(2,1)S(1)} fusion(f32[1024,384]{0,1:T(8,128)} %fusion.3, bf16[2048,1024]{1,0:T(8,128)(2,1)} %all-gather.3.cloned.1.call-done, bf16[1,384,2048]{2,1,0:T(8,128)(2,1)S(1)} %copy-done), kind=kOutput, calls=%fused_computation.11 | convolution fusion | flops 1612578816 | bytes 8126464 | tf_op jit(solution)/shard_map/dc,td->ct/dot_general | solution.py:50
  204.9 1.3 collective-permute-start
  206.5 0.8 collective-permute-start.7
  208.5 3.8 %fusion.16 = f32[8,52,1024]{2,0,1:T(8,128)S(1)} fusion(bf16[1024,1,7,30]{0,2,3,1:T(8,128)(2,1)S(1)} %slice.7, bf16[1024,1,8,52]{0,2,3,1:T(8,128)(2,1)S(1)} %copy.12, pred[8,52]{0,1:T(8,128)(4,1)S(1)} %copy-done.15, bf16[1024,1,31]{0,2,1:T(8,128)(2,1)S(1)} %bitcast.50), kind=kOutput, calls=%fused_computation.27 | convolution fusion | flops 31719424 | bytes 3049888 | tf_op jit(solution)/shard_map/conv_general_dilated | solution.py:18
  212.3 2.3 copy.14
  214.6 1.6 reshape.21
  220.9 1.4 convolution_dynamic-update-slice_fusion.1
  222.3 1.0 collective-permute-done.7
  223.3 1.4 convolution_dynamic-update-slice_fusion
  224.7 1.1 copy-done.1
  (56 shorter events, 6.7 us)
Async XLA Ops:
  6.5 120.8 %copy-start = (bf16[1,384,2048]{2,1,0:T(8,128)(2,1)S(1)}, bf16[1,384,2048]{2,1,0:T(8,128)(2,1)}, u32[]{:S(2)}) copy-start(bf16[1,384,2048]{2,1,0:T(8,128)(2,1)} %param.6) | copy-start | bytes 4718596
  6.5 120.8 %all-gather.5.cloned.1.call-start = ((), (), s32[]{:S(2)}) async-start(), calls=%async_computation.1 | async-start | bytes 4718592 | tf_op jit(solution)/shard_map/all_gather | solution.py:58
  7.3 193.1 %all-gather.3.cloned.1.call-start = ((), (), s32[]{:S(2)}) async-start(), calls=%async_computation | async-start | bytes 4718592 | tf_op jit(solution)/shard_map/all_gather | solution.py:52
  8.0 18.6 %collective-permute-start.1 = (bf16[1024,256]{1,0:T(8,128)(2,1)}, bf16[1024,256]{1,0:T(8,128)(2,1)S(1)}, u32[]{:S(2)}, u32[]{:S(2)}) collective-permute-start(bf16[1024,256]{1,0:T(8,128)(2,1)} %param.11), channel_id=1, source_target_pairs={{0,1},{1,2},{2,3},{3,4},{4,5},{5,6},{6,7},{7,0},{8,9},{9,10},{10,1... | collective-permute-start | bytes 1572872 | tf_op jit(solution)/shard_map/ppermute | solution.py:38
  26.6 0.9 copy-start.3
  27.5 26.9 %collective-permute-start.2 = (bf16[1024,256]{1,0:T(8,128)(2,1)S(1)}, bf16[1024,256]{1,0:T(8,128)(2,1)S(1)}, u32[]{:S(2)}, u32[]{:S(2)}) collective-permute-start(bf16[1024,256]{1,0:T(8,128)(2,1)S(1)} %collective-permute-done.1), channel_id=1, source_target_pairs={{0,1},{1,2},{2,3},{3,4},{4,5},{5,6},{6,7},{7,0},{8,9},{9,10},{10,1... | collective-permute-start | bytes 1572872 | tf_op jit(solution)/shard_map/ppermute | solution.py:38
  55.2 27.0 %collective-permute-start.3 = (bf16[1024,256]{1,0:T(8,128)(2,1)S(1)}, bf16[1024,256]{1,0:T(8,128)(2,1)S(1)}, u32[]{:S(2)}, u32[]{:S(2)}) collective-permute-start(bf16[1024,256]{1,0:T(8,128)(2,1)S(1)} %collective-permute-done.2), channel_id=1, source_target_pairs={{0,1},{1,2},{2,3},{3,4},{4,5},{5,6},{6,7},{7,0},{8,9},{9,10},{10,1... | collective-permute-start | bytes 1572872 | tf_op jit(solution)/shard_map/ppermute | solution.py:38
  82.9 26.9 %collective-permute-start.4 = (bf16[1024,256]{1,0:T(8,128)(2,1)S(1)}, bf16[1024,256]{1,0:T(8,128)(2,1)S(1)}, u32[]{:S(2)}, u32[]{:S(2)}) collective-permute-start(bf16[1024,256]{1,0:T(8,128)(2,1)S(1)} %collective-permute-done.3), channel_id=1, source_target_pairs={{0,1},{1,2},{2,3},{3,4},{4,5},{5,6},{6,7},{7,0},{8,9},{9,10},{10,1... | collective-permute-start | bytes 1572872 | tf_op jit(solution)/shard_map/ppermute | solution.py:38
  109.8 0.8 copy-start.9
  110.6 16.7 %collective-permute-start.5 = (bf16[1024,256]{1,0:T(8,128)(2,1)S(1)}, bf16[1024,256]{1,0:T(8,128)(2,1)S(1)}, u32[]{:S(2)}, u32[]{:S(2)}) collective-permute-start(bf16[1024,256]{1,0:T(8,128)(2,1)S(1)} %collective-permute-done.4), channel_id=1, source_target_pairs={{0,1},{1,2},{2,3},{3,4},{4,5},{5,6},{6,7},{7,0},{8,9},{9,10},{10,1... | collective-permute-start | bytes 1572872 | tf_op jit(solution)/shard_map/ppermute | solution.py:38
  127.3 5.4 %copy-start.11 = (bf16[1024,256]{1,0:T(8,128)(2,1)}, bf16[1024,256]{1,0:T(8,128)(2,1)S(1)}, u32[]{:S(2)}) copy-start(bf16[1024,256]{1,0:T(8,128)(2,1)S(1)} %collective-permute-done.5) | copy-start | bytes 1572868
  127.3 79.1 %collective-permute-start.6 = (bf16[1024,256]{1,0:T(8,128)(2,1)S(1)}, bf16[1024,256]{1,0:T(8,128)(2,1)}, u32[]{:S(2)}, u32[]{:S(2)}) collective-permute-start(bf16[1024,256]{1,0:T(8,128)(2,1)S(1)} %collective-permute-done.5), channel_id=1, source_target_pairs={{0,1},{1,2},{2,3},{3,4},{4,5},{5,6},{6,7},{7,0},{8,9},{9,10},{10,1... | collective-permute-start | bytes 1572872 | tf_op jit(solution)/shard_map/ppermute | solution.py:38
  132.7 73.6 %copy-start.13 = (bf16[1024]{0:T(1024)(128)(2,1)S(1)}, bf16[1024]{0:T(1024)(128)(2,1)}, u32[]{:S(2)}) copy-start(bf16[1024]{0:T(1024)(128)(2,1)} %param.10) | copy-start | bytes 6148
  204.9 2.3 collective-permute-start
  206.5 16.8 %collective-permute-start.7 = (bf16[1024,256]{1,0:T(8,128)(2,1)}, bf16[1024,256]{1,0:T(8,128)(2,1)}, u32[]{:S(2)}, u32[]{:S(2)}) collective-permute-start(bf16[1024,256]{1,0:T(8,128)(2,1)} %collective-permute-done.6), channel_id=1, source_target_pairs={{0,1},{1,2},{2,3},{3,4},{4,5},{5,6},{6,7},{7,0},{8,9},{9,10},{10,1... | collective-permute-start | bytes 1572872 | tf_op jit(solution)/shard_map/ppermute | solution.py:38
  207.7 0.8 copy-start.14
  207.7 0.8 copy-start.15
  216.6 1.1 copy-start.2
  217.2 1.1 copy-start.4
  217.7 1.1 copy-start.6
  218.3 1.1 copy-start.8
  218.8 1.1 copy-start.10
  219.4 1.1 copy-start.12
  224.7 1.1 copy-start.1
  (2 other events, 1.6 us)
Sparse Core Ops, SparseCore 0:
  9.5 101.6 all-gather.4
  113.3 87.0 all-gather.2
